TPU v7x, 32 devices: a whole 2x2x4 slice. The times are simulated.
32 devices in a mesh: ep: 8 (over z, x), tp: 4 (over y, core).
Axes of the slice: x: 2, y: 2, z: 4, core: 2. Of those that a mesh axis runs over, the one named last changes fastest.
Arguments:
- queries: bfloat16 [4096, 1024], P('ep', 'tp'), may hold values from -8 to 8
- keys_values: bfloat16 [4096, 1024], P('ep', 'tp'), may hold values from -60 to 60
- forget_cache: float32 [16, 4096], P('tp'), may hold values from -617 to 0, as said below
- heads_gain: float32 [1024], replicated, may hold values from 0.1 to 1.9
- output_weight: bfloat16 [1024, 2048], replicated, may hold values from -0.1875 to 0.1875
- expert_tokens: bfloat16 [1024, 2048], P('ep'), may hold values from -600 to 600
- expert_gain: float32 [2048], replicated, may hold values from 0.1 to 1.9
- routes: int32 [1024, 4], P('ep'), may hold values from 0 to 7, all different within a row; in each aligned block of 128 rows (0 to 127, 128 to 255, ...) at most 128 rows name the same one
- route_logits: float32 [1024, 4], P('ep'), may hold values from -6 to 301
- gate_weight: bfloat16 [8, 2048, 2048], P('ep', None, 'tp'), may hold values from -0.5 to 0.5
- up_weight: bfloat16 [8, 2048, 2048], P('ep', None, 'tp'), may hold values from -0.5 to 0.5
- down_weight: bfloat16 [8, 2048, 2048], P('ep', 'tp'), may hold values from -0.015625 to 0.015625
Outputs:
- mixer_out: bfloat16 [4096, 2048], P(('ep', 'tp'))
- moe_out: bfloat16 [1024, 2048], P('ep', 'tp')
Inputs may be any that keep to these rules, and one draw needn't show every extreme that they name: `forget_cache`: each row never rises from one position to the next. `routes`: the 4 experts of a row differ. In each aligned block of 128 rows (one device's tokens) no expert is named more than 128 times, so slot is below 128; some expert is named exactly 128 times in some block.
All inputs are finite; a program needn't handle non-finite values.
Results may differ from a plain program's by a relative error of at most 0.017.
Values may be sent and summed in bfloat16 or wider, within the bound.
A program may use at most 128 MiB of HBM per device.

v0:
```python
import math

import jax
import jax.numpy as jnp
from jax import lax
from jax.experimental import pallas as pl
from jax.experimental.pallas import tpu as pltpu
from jax.sharding import PartitionSpec as P

HEAD = 64


epsilon = 1e-06
clamp_limit = 7.0
sigmoid_slope = 1.702


def scaled_rows(values, gain_vector):
    as_float = values.astype(jnp.float32)
    inverse = lax.rsqrt(jnp.mean(as_float * as_float, axis=-1, keepdims=True) + epsilon)
    return (as_float * inverse * gain_vector).astype(jnp.bfloat16)


def assign_slots(routes, experts, capacity):
    row_count, pick_count = routes.shape
    flat_routes = routes.reshape(-1)
    onehot = (flat_routes[:, None] == jnp.arange(experts, dtype=jnp.int32)[None, :]).astype(
        jnp.int32
    )
    earlier = jnp.cumsum(onehot, axis=0) - onehot
    slot_rank = jnp.sum(earlier * onehot, axis=1)
    position = flat_routes * capacity + slot_rank
    owner_row = jnp.arange(row_count * pick_count, dtype=jnp.int32) // pick_count
    slot_token = jnp.full((experts * capacity,), row_count, jnp.int32).at[position].set(owner_row)
    return (position.reshape(row_count, pick_count), slot_token)


def body(
    queries,
    keys_values,
    forget_cache,
    heads_gain,
    output_weight,
    expert_tokens,
    expert_gain,
    routes,
    route_logits,
    gate_weight,
    up_weight,
    down_weight,
):
    row_count = queries.shape[0]
    query_count = queries.shape[1] // HEAD
    key_count = keys_values.shape[1] // (2 * HEAD)
    group_size = query_count // key_count
    offset = lax.axis_index("ep") * row_count
    score_scale = 1.0 / math.sqrt(HEAD)
    count_rows = queries.shape[0]
    segment_positions = offset + jnp.arange(count_rows, dtype=jnp.int32)
    gate_rows = lax.dynamic_slice_in_dim(forget_cache, offset, count_rows, 1)
    segment_bias = gate_rows.T.reshape(count_rows, key_count, group_size, 1)
    segments = [
        (queries.reshape(count_rows, key_count, group_size, HEAD), segment_positions, segment_bias)
    ]
    start_states = tuple(
        [
            (
                jnp.full((grouped.shape[0], key_count, group_size), -jnp.inf, jnp.float32),
                jnp.zeros((grouped.shape[0], key_count, group_size), jnp.float32),
                jnp.zeros((grouped.shape[0], key_count, group_size, HEAD), jnp.float32),
            )
            for grouped, positions, bias in segments
        ]
    )
    piece_rows = lax.all_gather(
        keys_values.reshape(row_count, key_count, 2 * HEAD), "ep", axis=0, tiled=True
    )
    count_rows = piece_rows.shape[0]
    block_width = 512
    blocks = piece_rows.reshape(count_rows // block_width, block_width, key_count, 2 * HEAD)

    def one_block(states, scan_item):
        block_rows, block_index = scan_item
        first_key = block_index * block_width
        key_block = block_rows[:, :, :HEAD]
        value_block = block_rows[:, :, HEAD:]
        key_gate = lax.dynamic_slice_in_dim(forget_cache, first_key, block_width, 1).reshape(
            1, key_count, group_size, block_width
        )
        key_pos = first_key + jnp.arange(block_width, dtype=jnp.int32)
        updated = []
        for (grouped, positions, bias), state in zip(segments, states):

            def take_block(state_in, grouped=grouped, positions=positions, bias=bias):
                running_max, running_sum, weighted = state_in
                scores = (
                    jnp.einsum(
                        "qhgd,khd->qhgk", grouped, key_block, preferred_element_type=jnp.float32
                    )
                    * score_scale
                )
                scores = scores + bias - key_gate
                visible = (key_pos[None, :] <= positions[:, None])[:, None, None, :]
                scores = jnp.where(visible, scores, -jnp.inf)
                new_max = jnp.maximum(running_max, jnp.max(scores, axis=-1))
                safe_max = jnp.where(jnp.isfinite(new_max), new_max, 0.0)
                factor = jnp.exp(running_max - safe_max)
                weights = jnp.exp(scores - safe_max[..., None])
                running_sum = running_sum * factor + jnp.sum(weights, axis=-1)
                weighted = weighted * factor[..., None] + jnp.einsum(
                    "qhgk,khd->qhgd",
                    weights.astype(jnp.bfloat16),
                    value_block,
                    preferred_element_type=jnp.float32,
                )
                return (new_max, running_sum, weighted)

            def keep_state(state_in):
                return state_in

            updated.append(lax.cond(first_key <= positions[-1], take_block, keep_state, state))
        return (tuple(updated), None)

    final_states, _ = lax.scan(
        one_block, start_states, (blocks, jnp.arange(count_rows // block_width, dtype=jnp.int32))
    )
    outputs = [
        (weighted / running_sum[..., None])
        .reshape(running_sum.shape[0], query_count * HEAD)
        .astype(jnp.bfloat16)
        for running_max, running_sum, weighted in final_states
    ]
    attended = outputs[0]
    local_rows = lax.all_to_all(attended, "tp", split_axis=0, concat_axis=1, tiled=True)
    heads_normed = scaled_rows(local_rows, heads_gain)
    mixer_out = jnp.dot(heads_normed, output_weight, preferred_element_type=jnp.float32).astype(
        jnp.bfloat16
    )
    experts_count = lax.axis_size("ep")
    expert_rows, pick_count = routes.shape
    capacity = 2 * expert_rows * pick_count // experts_count
    expert_in = scaled_rows(expert_tokens, expert_gain)
    shifted = route_logits - jnp.max(route_logits, axis=1, keepdims=True)
    raised = jnp.exp(shifted)
    route_weight = raised / jnp.sum(raised, axis=1, keepdims=True)
    position, slot_token = assign_slots(routes, experts_count, capacity)
    model_width = expert_in.shape[1]
    part_width = model_width // lax.axis_size("tp")
    gate_local = gate_weight[0]
    up_local = up_weight[0]
    down_local = down_weight[0]
    own_columns = lax.dynamic_slice_in_dim(
        expert_in, lax.axis_index("tp") * part_width, part_width, 1
    )
    padded = jnp.concatenate([own_columns, jnp.zeros((1, part_width), jnp.bfloat16)], axis=0)
    outgoing = jnp.take(padded, slot_token, axis=0).reshape(experts_count, capacity, part_width)
    arrived = lax.all_to_all(outgoing, "ep", split_axis=0, concat_axis=0, tiled=True).reshape(
        experts_count * capacity, part_width
    )
    piece_rows = lax.all_gather(arrived, "tp", axis=1, tiled=True)
    gate_sum = jnp.dot(piece_rows, gate_local, preferred_element_type=jnp.float32)
    up_sum = jnp.dot(piece_rows, up_local, preferred_element_type=jnp.float32)
    gate_cut = jnp.minimum(gate_sum, clamp_limit)
    up_cut = jnp.clip(up_sum, -clamp_limit, clamp_limit)
    hidden = ((up_cut + 1.0) * gate_cut * jax.nn.sigmoid(sigmoid_slope * gate_cut)).astype(
        jnp.bfloat16
    )
    expert_out = lax.psum_scatter(
        lax.dot_general(
            down_local, hidden, (((0,), (1,)), ((), ())), preferred_element_type=jnp.float32
        ).astype(jnp.bfloat16),
        "tp",
        scatter_dimension=0,
        tiled=True,
    )
    returned = lax.all_to_all(expert_out, "ep", split_axis=1, concat_axis=1, tiled=True)
    picked = jnp.take(returned, position.reshape(-1), axis=1).reshape(
        part_width, expert_rows, pick_count
    )
    moe_out = jnp.einsum("crk,rk->rc", picked.astype(jnp.float32), route_weight).astype(
        jnp.bfloat16
    )
    return (mixer_out, moe_out)


MESH = pl.DeviceIdType.MESH


def fused_kernel(
    E,
    T,
    loads,
    q_ref,
    kv_ref,
    f_ref,
    hg_ref,
    ow_hbm,
    tok_ref,
    eg_ref,
    routes_ref,
    logits_ref,
    gw_hbm,
    uw_hbm,
    dw_hbm,
    mix_ref,
    moe_ref,
    ow,
    gw,
    uw,
    dw,
    normed,
    tokall,
    kvall,
    qs,
    m_sc,
    acc_sc,
    s1s,
    s1r,
    s1o,
    s2s,
    s2r,
    s2o,
    s3s,
    s3r,
    att,
    attall,
    wsem,
    ssem,
    tok_rs,
    kv_rs,
    s1_rs,
    s2_rs,
    s3_rs,
    att_rs,
):
    f32, bf16 = jnp.float32, jnp.bfloat16
    e = lax.axis_index("ep")
    t = lax.axis_index("tp")
    B = 1
    while 4 * B * B <= E:
        B *= 2
    A = E // B
    Y = T // 2
    a, b = e // B, e % B
    y, c = t // 2, t % 2
    mate = y * 2 + (1 - c)
    rows = q_ref.shape[0]
    heads = q_ref.shape[1] // HEAD
    kv_heads = kv_ref.shape[1] // (2 * HEAD)
    group = heads // kv_heads
    erows, width = tok_ref.shape
    part = width // T

    weight_copies = [
        pltpu.make_async_copy(gw_hbm.at[0], gw, wsem.at[0]),
        pltpu.make_async_copy(uw_hbm.at[0], uw, wsem.at[1]),
        pltpu.make_async_copy(dw_hbm.at[0], dw, wsem.at[2]),
        pltpu.make_async_copy(ow_hbm, ow, wsem.at[3]),
    ]
    for copy in loads + weight_copies:
        copy.start()

    barrier = pltpu.get_barrier_semaphore()
    for d in range(1, E):
        pl.semaphore_signal(barrier, inc=1, device_id=(lax.rem(e + d, E), t), device_id_type=MESH)
    for d in range(1, T):
        pl.semaphore_signal(barrier, inc=1, device_id=(e, lax.rem(t + d, T)), device_id_type=MESH)

    for copy in loads:
        copy.wait()
    tokens = tok_ref[...].astype(f32)
    inverse = lax.rsqrt(jnp.mean(tokens * tokens, axis=-1, keepdims=True) + epsilon)
    in_rows = (tokens * inverse * eg_ref[...]).astype(bf16)
    for quarter in range(T):
        normed[quarter] = in_rows[:, quarter * part : (quarter + 1) * part]
        tokall[quarter, e] = in_rows[:, quarter * part : (quarter + 1) * part]
    for h in range(heads):
        qs[h] = jnp.concatenate(
            [q_ref[:, h * HEAD : (h + 1) * HEAD] * jnp.asarray(0.125, bf16), jnp.zeros((rows, HEAD), bf16)],
            axis=1,
        )
    pl.semaphore_wait(barrier, E - 1 + T - 1)

    sent = []

    def send(cond, src, dst, recv, device):
        slot = len(sent)

        def build():
            return pltpu.make_async_remote_copy(
                src_ref=src, dst_ref=dst, send_sem=ssem.at[slot], recv_sem=recv,
                device_id=device, device_id_type=MESH,
            )

        sent.append((cond, build))
        if cond is None:
            build().start()
        else:
            @pl.when(cond)
            def _():
                build().start()

    def arrive(cond, dst, recv):
        def go():
            pltpu.make_async_remote_copy(
                src_ref=dst, dst_ref=dst, send_sem=ssem.at[0], recv_sem=recv,
                device_id=(e, mate), device_id_type=MESH,
            ).wait_recv()

        if cond is None:
            go()
        else:
            pl.when(cond)(go)

    def both(p, q):
        return q if p is None else (p if q is None else jnp.logical_and(p, q))

    def send_token_block(cond, j, up, down, across):
        src = tokall.at[t, j]
        if j is e:
            src = normed.at[t]
        dst, recv = tokall.at[t, j], tok_rs.at[j, t]
        if up:
            send(both(cond, a + 1 < A), src, dst, recv, (e + B, t))
        if down:
            send(both(cond, a > 0), src, dst, recv, (e - B, t))
        if across:
            for d in range(1, B):
                send(cond, src, dst, recv, (a * B + lax.rem(b + d, B), t))
        if j is not e:
            for d in range(1, Y):
                send(cond, src, dst, recv, (e, lax.rem(y + d, Y) * 2 + c))
            send(cond, src, dst, recv, (e, mate))

    def send_kv_block(cond, j):
        src = kv_ref if j is e else kvall.at[j]
        dst, recv = kvall.at[j], kv_rs.at[j]
        send(both(cond, a + 1 < A), src, dst, recv, (e + B, t))
        for d in range(1, B):
            ob = lax.rem(b + d, B)
            wanted = a * B + ob > j
            send(both(cond, wanted), src, dst, recv, (a * B + ob, t))

    def attend(block, j, diag):
        def head_body(h, carry):
            kv_off = pl.multiple_of((h // group) * 2 * HEAD, 2 * HEAD)
            kvb = block[:, pl.ds(kv_off, 2 * HEAD)]
            lane = lax.broadcasted_iota(jnp.int32, kvb.shape, 1)
            vaug = jnp.where(lane < HEAD, jnp.asarray(1.0, bf16), kvb)
            fk = f_ref[pl.ds(h, 1), pl.ds(pl.multiple_of(j * rows, rows), rows)]
            half = rows // 2
            for r in range(2):
                rs = slice(r * half, (r + 1) * half)
                klen = half * (r + 1) if diag else rows
                s = lax.dot_general(
                    qs[h, rs], kvb[:klen], (((1,), (1,)), ((), ())), preferred_element_type=f32
                )
                s = s - fk[:, :klen]
                if diag:
                    qp = lax.broadcasted_iota(jnp.int32, s.shape, 0) + r * half
                    kp = lax.broadcasted_iota(jnp.int32, s.shape, 1)
                    s = jnp.where(kp <= qp, s, -jnp.inf)
                top = jnp.max(s, axis=1, keepdims=True)
                if not diag:
                    old = m_sc[h, rs][:, :1]
                    top = jnp.maximum(top, old)
                p = jnp.exp(s - top).astype(bf16)
                pv = jnp.dot(p, vaug[:klen], preferred_element_type=f32)
                if not diag:
                    pv = acc_sc[h, rs] * jnp.exp(old - top) + pv
                acc_sc[h, rs] = pv
                m_sc[h, rs] = jnp.broadcast_to(top, (half, 128))
            return carry

        lax.fori_loop(0, heads, head_body, 0)

    send_token_block(None, e, True, True, True)
    send_kv_block(None, e)
    attend(kv_ref, e, True)

    def y_forward(cond, j):
        for d in range(1, Y):
            oy = lax.rem(y + d, Y) * 2 + c
            arrive(cond, tokall.at[oy, j], tok_rs.at[j, oy])
            send(cond, tokall.at[oy, j], tokall.at[oy, j], tok_rs.at[j, oy], (e, mate))

    late = []
    for s in range(1, A + 2):
        pending = late
        late = []
        if s < A:
            up_ok, down_ok = a - s >= 0, a + s < A
            ju, jd = e - s * B, e + s * B
            arrive(up_ok, tokall.at[t, ju], tok_rs.at[ju, t])
            send_token_block(up_ok, ju, True, False, True)
            arrive(down_ok, tokall.at[t, jd], tok_rs.at[jd, t])
            send_token_block(down_ok, jd, False, True, True)
            late += [(up_ok, ju), (down_ok, jd)]
            arrive(up_ok, kvall.at[ju], kv_rs.at[ju])
            send_kv_block(up_ok, ju)
        if s <= A:
            for d in range(1, B):
                ob = lax.rem(b + d, B)
                for sign in (1, -1) if s > 1 else (1,):
                    oa = a - sign * (s - 1)
                    ok = None if s == 1 else (oa >= 0 if sign == 1 else oa < A)
                    j = oa * B + ob
                    arrive(ok, tokall.at[t, j], tok_rs.at[j, t])
                    send_token_block(ok, j, False, False, False)
                    late.append((ok, j))
        for cond, j in pending:
            y_forward(cond, j)
        if s < A:
            ju = e - s * B

            @pl.when(a - s >= 0)
            def _(ju=ju):
                attend(kvall.at[ju], ju, False)

    for copy in weight_copies[:3]:
        copy.wait()

    chunks, cb = A, B
    crows = cb * erows

    def first_block(i):
        return lax.rem(a + i + 1, A) * cb

    side = []
    for d in range(1, B):
        ob = lax.rem(b + d, B)
        for s in range(A):
            side.append((jnp.logical_and(a - s >= 0, (a - s) * B + ob < e), (a - s) * B + ob))

    def side_step():
        if side:
            cond, j = side.pop(0)

            @pl.when(cond)
            def _():
                arrive(None, kvall.at[j], kv_rs.at[j])
                attend(kvall.at[j], j, False)

    def expert_chunk(i):
        start = first_block(i)
        for k in range(cb):
            for oy in range(Y):
                quarter = oy * 2 + (1 - c)
                arrive(
                    start + k != e, tokall.at[quarter, start + k], tok_rs.at[start + k, quarter]
                )
        x = jnp.concatenate(
            [tokall[qt, pl.ds(start, cb)].reshape(crows, part) for qt in range(T)], axis=1
        )
        gate = jnp.dot(x, gw[...], preferred_element_type=f32)
        up = jnp.dot(x, uw[...], preferred_element_type=f32)
        gate = jnp.minimum(gate, clamp_limit)
        up = jnp.clip(up, -clamp_limit, clamp_limit)
        hidden = ((up + 1.0) * gate * jax.nn.sigmoid(sigmoid_slope * gate)).astype(bf16)
        for oy in range(Y):
            for oc in range(2):
                col = (oy * 2 + oc) * part
                out = jnp.dot(hidden, dw[:, col : col + part], preferred_element_type=f32).astype(bf16)

                @pl.when(c == oc)
                def _():
                    s1o[i, oy] = out

                @pl.when(c != oc)
                def _():
                    s1s[i, oy] = out

        send(None, s1s.at[i], s1r.at[i], s1_rs.at[i], (e, mate))

    def reduce_pair(i):
        arrive(None, s1r.at[i], s1_rs.at[i])
        for oy in range(Y):
            out = (s1o[i, oy].astype(f32) + s1r[i, oy].astype(f32)).astype(bf16)

            @pl.when(y == oy)
            def _():
                s2o[i] = out

            @pl.when(y != oy)
            def _():
                s2s[i, oy] = out

        for d in range(1, Y):
            oy = lax.rem(y + d, Y)
            send(None, s2s.at[i, oy], s2r.at[i, y], s2_rs.at[i, y], (e, oy * 2 + c))

    def reduce_rest(i):
        total = s2o[i].astype(f32)
        for d in range(1, Y):
            oy = lax.rem(y + d, Y)
            arrive(None, s2r.at[i, oy], s2_rs.at[i, oy])
            total = total + s2r[i, oy].astype(f32)
        total = total.astype(bf16)
        for k in range(cb):
            j = first_block(i) + k
            out = total[k * erows : (k + 1) * erows]
            s3s[j] = out

            @pl.when(e == j)
            def _():
                s3r[j] = out

        for k in range(cb):
            j = first_block(i) + k
            send(e != j, s3s.at[j], s3r.at[e], s3_rs.at[e], (j, t))

    for i in range(chunks + 2):
        if i < chunks:
            expert_chunk(i)
        if 1 <= i <= chunks:
            reduce_pair(i - 1)
        if i >= 1:
            side_step()
        if i >= 2:
            reduce_rest(i - 2)
    while side:
        side_step()

    arows = rows // T
    for h in range(heads):
        acc = acc_sc[h]
        out = (acc[:, HEAD:] / acc[:, :HEAD]).astype(bf16)
        for tt in range(T):
            att[tt, :, h * HEAD : (h + 1) * HEAD] = out[tt * arows : (tt + 1) * arows]
    attall[t] = att[t]
    for d in range(1, T):
        ot = lax.rem(t + d, T)
        send(None, att.at[ot], attall.at[t], att_rs.at[t], (e, ot))
    weight_copies[3].wait()
    for d in range(1, T):
        ot = lax.rem(t + d, T)
        arrive(None, attall.at[ot], att_rs.at[ot])
    mixed = jnp.concatenate([attall[tt] for tt in range(T)], axis=1).astype(f32)
    inverse = lax.rsqrt(jnp.mean(mixed * mixed, axis=-1, keepdims=True) + epsilon)
    mixed = (mixed * inverse * hg_ref[...]).astype(bf16)
    mix_ref[...] = jnp.dot(mixed, ow[...], preferred_element_type=f32).astype(bf16)

    logits = logits_ref[...]
    raised = jnp.exp(logits - jnp.max(logits, axis=0, keepdims=True))
    weight = raised / jnp.sum(raised, axis=0, keepdims=True)
    chosen = routes_ref[...]
    table = jnp.concatenate(
        [jnp.sum(jnp.where(chosen == j, weight, 0.0), axis=0, keepdims=True) for j in range(E)],
        axis=0,
    ).T
    for d in range(1, E):
        j = lax.rem(e + d, E)
        arrive(None, s3r.at[j], s3_rs.at[j])
    total = jnp.zeros((erows, part), f32)
    for j in range(E):
        total = total + s3r[j].astype(f32) * table[:, j : j + 1]
    moe_ref[...] = total.astype(bf16)

    for cond, build in sent:
        if cond is None:
            build().wait_send()
        else:
            @pl.when(cond)
            def _():
                build().wait_send()


def fused_body(*args):
    (queries, keys_values, forget_cache, heads_gain, output_weight, expert_tokens,
     expert_gain, routes, route_logits, gate_weight, up_weight, down_weight) = args
    E, T = lax.axis_size("ep"), lax.axis_size("tp")
    rows = queries.shape[0]
    heads = queries.shape[1] // HEAD
    erows, width = expert_tokens.shape
    part = width // T
    ff = gate_weight.shape[2]
    B = 1
    while 4 * B * B <= E:
        B *= 2
    chunks = E // B
    crows = B * erows
    Y = T // 2
    bf16, f32 = jnp.bfloat16, jnp.float32
    V, DMA = pltpu.VMEM, pltpu.SemaphoreType.DMA
    vm = pl.BlockSpec(memory_space=pltpu.VMEM)
    hbm = pl.BlockSpec(memory_space=pltpu.HBM)

    operands = [
        queries, keys_values, forget_cache, heads_gain.reshape(1, -1), output_weight, expert_tokens,
        expert_gain.reshape(1, -1), routes.T, route_logits.T, gate_weight, up_weight, down_weight,
    ]
    small = [5, 6, 1, 0, 2, 3, 7, 8]

    def kernel(*refs):
        refs = list(refs)
        load_sem = refs.pop()
        held = refs[-len(small) :]
        refs = refs[: -len(small)]
        loads = []
        for n, (index, place) in enumerate(zip(small, held)):
            loads.append(pltpu.make_async_copy(refs[index], place, load_sem.at[n]))
            refs[index] = place
        fused_kernel(E, T, loads, *refs)

    return pl.pallas_call(
        kernel,
        out_shape=(
            jax.ShapeDtypeStruct((rows // T, output_weight.shape[1]), bf16),
            jax.ShapeDtypeStruct((erows, part), bf16),
        ),
        in_specs=[hbm] * len(operands),
        out_specs=(vm, vm),
        scratch_shapes=[
            V(output_weight.shape, bf16),
            V(gate_weight.shape[1:], bf16),
            V(up_weight.shape[1:], bf16),
            V(down_weight.shape[1:], bf16),
            V((T, erows, part), bf16),
            V((T, E, erows, part), bf16),
            V((E,) + keys_values.shape, bf16),
            V((heads, rows, 2 * HEAD), bf16),
            V((heads, rows, 128), f32),
            V((heads, rows, 2 * HEAD), f32),
            V((chunks, Y, crows, part), bf16),
            V((chunks, Y, crows, part), bf16),
            V((chunks, Y, crows, part), bf16),
            V((chunks, Y, crows, part), bf16),
            V((chunks, Y, crows, part), bf16),
            V((chunks, crows, part), bf16),
            V((E, erows, part), bf16),
            V((E, erows, part), bf16),
            V((T, rows // T, queries.shape[1]), bf16),
            V((T, rows // T, queries.shape[1]), bf16),
            DMA((4,)),
            DMA((128,)),
            DMA((E, T)),
            DMA((E,)),
            DMA((chunks,)),
            DMA((chunks, Y)),
            DMA((E,)),
            DMA((T,)),
        ]
        + [V(operands[n].shape, operands[n].dtype) for n in small]
        + [DMA((len(small),))],
        compiler_params=pltpu.CompilerParams(
            collective_id=0, has_side_effects=True, vmem_limit_bytes=60 * 1024 * 1024
        ),
    )(*operands)


def pick_body(*args):
    routes = args[7]
    rows, picks = routes.shape
    capacity = 2 * rows * picks // lax.axis_size("ep")
    if capacity >= rows and lax.axis_size("tp") % 2 == 0:
        return fused_body(*args)
    return body(*args)


def solution(mesh):
    placed = (
        P("ep", "tp"),
        P("ep", "tp"),
        P("tp", None),
        P(),
        P(),
        P("ep", None),
        P(),
        P("ep", None),
        P("ep", None),
        P("ep", None, "tp"),
        P("ep", None, "tp"),
        P("ep", "tp", None),
    )
    return jax.shard_map(
        pick_body,
        mesh=mesh,
        in_specs=placed,
        out_specs=(P(("ep", "tp"), None), P("ep", "tp")),
        check_vma=False,
    )
```

profile of v0, /device:TPU:10, one launch (start us, length us, event | category | flops | bytes accessed | tf_op | source)
XLA Modules:
  0.0 87.4 jit_solution(889844413718631190)
XLA Ops:
  0.6 83.3 %shard_map.131 = (bf16[128,2048]{1,0:T(8,128)(2,1)}, bf16[128,512]{1,0:T(8,128)(2,1)}) custom-call(bf16[512,256]{1,0:T(8,128)(2,1)} %refs_0_.1, bf16[512,256]{1,0:T(8,128)(2,1)} %refs_1_.1, f32[4,4096]{1,0:T(4,128)} %refs_2_.1, f32[1,1024]{1,0:T(1,128)} %bitcast.5, bf16[1024,2048]{1,0:T(8,128)(2,1)} %refs_4_.1, bf16[128,2048]{1,0:T(8,128)(2,1)} %refs_5_.1, ...), custom_call_target="tpu_custom_call" | custom-call | tf_op jit(solution)/shard_map/pallas_call | solution.py:605
  83.9 1.9 %copy.16 = bf16[128,2048]{1,0:T(8,128)(2,1)} copy(bf16[128,2048]{1,0:T(8,128)(2,1)} %get-tuple-element.4) | data formatting | bytes 1048576
  85.8 1.6 %copy.17 = bf16[128,512]{1,0:T(8,128)(2,1)} copy(bf16[128,512]{1,0:T(8,128)(2,1)} %get-tuple-element.5) | data formatting | bytes 262144
where the time goes:
time: 87.5 us; the launch traced here: 87.4 us
  Pallas kernels  83.3 us (95%)
  local copies, waits for them, and re-layouts  3.45 us (4%)
    pallas_call x1, Pallas kernels, fused_body(): pl.pallas_call(kernel, out_shape=(jax.ShapeDtypeStruct((rows // T, output...  83.3 us
    unnamed x2, local copies, waits for them, and re-layouts  3.45 us

commit v1 on v0

v1 whole, which is shorter than its diff:
```python
import math

import jax
import jax.numpy as jnp
from jax import lax
from jax.experimental import pallas as pl
from jax.experimental.pallas import tpu as pltpu
from jax.sharding import PartitionSpec as P

HEAD = 64


epsilon = 1e-06
clamp_limit = 7.0
sigmoid_slope = 1.702


def scaled_rows(values, gain_vector):
    as_float = values.astype(jnp.float32)
    inverse = lax.rsqrt(jnp.mean(as_float * as_float, axis=-1, keepdims=True) + epsilon)
    return (as_float * inverse * gain_vector).astype(jnp.bfloat16)


def assign_slots(routes, experts, capacity):
    row_count, pick_count = routes.shape
    flat_routes = routes.reshape(-1)
    onehot = (flat_routes[:, None] == jnp.arange(experts, dtype=jnp.int32)[None, :]).astype(
        jnp.int32
    )
    earlier = jnp.cumsum(onehot, axis=0) - onehot
    slot_rank = jnp.sum(earlier * onehot, axis=1)
    position = flat_routes * capacity + slot_rank
    owner_row = jnp.arange(row_count * pick_count, dtype=jnp.int32) // pick_count
    slot_token = jnp.full((experts * capacity,), row_count, jnp.int32).at[position].set(owner_row)
    return (position.reshape(row_count, pick_count), slot_token)


def body(
    queries,
    keys_values,
    forget_cache,
    heads_gain,
    output_weight,
    expert_tokens,
    expert_gain,
    routes,
    route_logits,
    gate_weight,
    up_weight,
    down_weight,
):
    row_count = queries.shape[0]
    query_count = queries.shape[1] // HEAD
    key_count = keys_values.shape[1] // (2 * HEAD)
    group_size = query_count // key_count
    offset = lax.axis_index("ep") * row_count
    score_scale = 1.0 / math.sqrt(HEAD)
    count_rows = queries.shape[0]
    segment_positions = offset + jnp.arange(count_rows, dtype=jnp.int32)
    gate_rows = lax.dynamic_slice_in_dim(forget_cache, offset, count_rows, 1)
    segment_bias = gate_rows.T.reshape(count_rows, key_count, group_size, 1)
    segments = [
        (queries.reshape(count_rows, key_count, group_size, HEAD), segment_positions, segment_bias)
    ]
    start_states = tuple(
        [
            (
                jnp.full((grouped.shape[0], key_count, group_size), -jnp.inf, jnp.float32),
                jnp.zeros((grouped.shape[0], key_count, group_size), jnp.float32),
                jnp.zeros((grouped.shape[0], key_count, group_size, HEAD), jnp.float32),
            )
            for grouped, positions, bias in segments
        ]
    )
    piece_rows = lax.all_gather(
        keys_values.reshape(row_count, key_count, 2 * HEAD), "ep", axis=0, tiled=True
    )
    count_rows = piece_rows.shape[0]
    block_width = 512
    blocks = piece_rows.reshape(count_rows // block_width, block_width, key_count, 2 * HEAD)

    def one_block(states, scan_item):
        block_rows, block_index = scan_item
        first_key = block_index * block_width
        key_block = block_rows[:, :, :HEAD]
        value_block = block_rows[:, :, HEAD:]
        key_gate = lax.dynamic_slice_in_dim(forget_cache, first_key, block_width, 1).reshape(
            1, key_count, group_size, block_width
        )
        key_pos = first_key + jnp.arange(block_width, dtype=jnp.int32)
        updated = []
        for (grouped, positions, bias), state in zip(segments, states):

            def take_block(state_in, grouped=grouped, positions=positions, bias=bias):
                running_max, running_sum, weighted = state_in
                scores = (
                    jnp.einsum(
                        "qhgd,khd->qhgk", grouped, key_block, preferred_element_type=jnp.float32
                    )
                    * score_scale
                )
                scores = scores + bias - key_gate
                visible = (key_pos[None, :] <= positions[:, None])[:, None, None, :]
                scores = jnp.where(visible, scores, -jnp.inf)
                new_max = jnp.maximum(running_max, jnp.max(scores, axis=-1))
                safe_max = jnp.where(jnp.isfinite(new_max), new_max, 0.0)
                factor = jnp.exp(running_max - safe_max)
                weights = jnp.exp(scores - safe_max[..., None])
                running_sum = running_sum * factor + jnp.sum(weights, axis=-1)
                weighted = weighted * factor[..., None] + jnp.einsum(
                    "qhgk,khd->qhgd",
                    weights.astype(jnp.bfloat16),
                    value_block,
                    preferred_element_type=jnp.float32,
                )
                return (new_max, running_sum, weighted)

            def keep_state(state_in):
                return state_in

            updated.append(lax.cond(first_key <= positions[-1], take_block, keep_state, state))
        return (tuple(updated), None)

    final_states, _ = lax.scan(
        one_block, start_states, (blocks, jnp.arange(count_rows // block_width, dtype=jnp.int32))
    )
    outputs = [
        (weighted / running_sum[..., None])
        .reshape(running_sum.shape[0], query_count * HEAD)
        .astype(jnp.bfloat16)
        for running_max, running_sum, weighted in final_states
    ]
    attended = outputs[0]
    local_rows = lax.all_to_all(attended, "tp", split_axis=0, concat_axis=1, tiled=True)
    heads_normed = scaled_rows(local_rows, heads_gain)
    mixer_out = jnp.dot(heads_normed, output_weight, preferred_element_type=jnp.float32).astype(
        jnp.bfloat16
    )
    experts_count = lax.axis_size("ep")
    expert_rows, pick_count = routes.shape
    capacity = 2 * expert_rows * pick_count // experts_count
    expert_in = scaled_rows(expert_tokens, expert_gain)
    shifted = route_logits - jnp.max(route_logits, axis=1, keepdims=True)
    raised = jnp.exp(shifted)
    route_weight = raised / jnp.sum(raised, axis=1, keepdims=True)
    position, slot_token = assign_slots(routes, experts_count, capacity)
    model_width = expert_in.shape[1]
    part_width = model_width // lax.axis_size("tp")
    gate_local = gate_weight[0]
    up_local = up_weight[0]
    down_local = down_weight[0]
    own_columns = lax.dynamic_slice_in_dim(
        expert_in, lax.axis_index("tp") * part_width, part_width, 1
    )
    padded = jnp.concatenate([own_columns, jnp.zeros((1, part_width), jnp.bfloat16)], axis=0)
    outgoing = jnp.take(padded, slot_token, axis=0).reshape(experts_count, capacity, part_width)
    arrived = lax.all_to_all(outgoing, "ep", split_axis=0, concat_axis=0, tiled=True).reshape(
        experts_count * capacity, part_width
    )
    piece_rows = lax.all_gather(arrived, "tp", axis=1, tiled=True)
    gate_sum = jnp.dot(piece_rows, gate_local, preferred_element_type=jnp.float32)
    up_sum = jnp.dot(piece_rows, up_local, preferred_element_type=jnp.float32)
    gate_cut = jnp.minimum(gate_sum, clamp_limit)
    up_cut = jnp.clip(up_sum, -clamp_limit, clamp_limit)
    hidden = ((up_cut + 1.0) * gate_cut * jax.nn.sigmoid(sigmoid_slope * gate_cut)).astype(
        jnp.bfloat16
    )
    expert_out = lax.psum_scatter(
        lax.dot_general(
            down_local, hidden, (((0,), (1,)), ((), ())), preferred_element_type=jnp.float32
        ).astype(jnp.bfloat16),
        "tp",
        scatter_dimension=0,
        tiled=True,
    )
    returned = lax.all_to_all(expert_out, "ep", split_axis=1, concat_axis=1, tiled=True)
    picked = jnp.take(returned, position.reshape(-1), axis=1).reshape(
        part_width, expert_rows, pick_count
    )
    moe_out = jnp.einsum("crk,rk->rc", picked.astype(jnp.float32), route_weight).astype(
        jnp.bfloat16
    )
    return (mixer_out, moe_out)


MESH = pl.DeviceIdType.MESH


def fused_kernel(
    E, T, loads,
    q_ref, kv_ref, f_ref, hg_ref, ow_hbm, tok_ref, eg_ref, routes_ref, logits_ref,
    gw_hbm, uw_hbm, dw_hbm,
    mix_ref, moe_ref,
    ow, gw, uw, dw, tokall, kvall, qa, fa, m_sc, acc_sc,
    s1s, s1r, s1o, s2s, s2r, s3s, s3r, zs, zr, wtab, att, attall,
    wsem, ssem, tok_rs, kv_rs, s1_rs, s2_rs, s3_rs, z_rs, wt_rs, att_rs,
):
    f32, bf16 = jnp.float32, jnp.bfloat16
    e = lax.axis_index("ep")
    t = lax.axis_index("tp")
    B = 2
    A = E // B
    a, b = e // B, e % B
    y, c = t // 2, t % 2
    mate = y * 2 + (1 - c)
    across_y = (1 - y) * 2 + c
    across_x = a * B + (1 - b)
    rows = q_ref.shape[0]
    heads = q_ref.shape[1] // HEAD
    kv_heads = kv_ref.shape[1] // (2 * HEAD)
    group = heads // kv_heads
    erows, width = tok_ref.shape
    part = width // T
    lanes = 2 * HEAD

    weight_copies = [
        pltpu.make_async_copy(gw_hbm.at[0], gw, wsem.at[0]),
        pltpu.make_async_copy(uw_hbm.at[0], uw, wsem.at[1]),
        pltpu.make_async_copy(dw_hbm.at[0], dw, wsem.at[2]),
        pltpu.make_async_copy(ow_hbm, ow, wsem.at[3]),
    ]
    for copy in loads:
        copy.start()

    barrier = pltpu.get_barrier_semaphore()
    for d in range(1, E):
        pl.semaphore_signal(barrier, inc=1, device_id=(lax.rem(e + d, E), t), device_id_type=MESH)
    for d in range(1, T):
        pl.semaphore_signal(barrier, inc=1, device_id=(e, lax.rem(t + d, T)), device_id_type=MESH)

    for copy in loads:
        copy.wait()
    for copy in weight_copies:
        copy.start()

    tokens = tok_ref[...].astype(f32)
    inverse = lax.rsqrt(jnp.mean(tokens * tokens, axis=-1, keepdims=True) + epsilon)
    in_rows = (tokens * inverse * eg_ref[...]).astype(bf16)
    for quarter in range(T):
        tokall[quarter, e] = in_rows[:, quarter * part : (quarter + 1) * part]
    logits = logits_ref[...]
    raised = jnp.exp(logits - jnp.max(logits, axis=0, keepdims=True))
    weight = raised / jnp.sum(raised, axis=0, keepdims=True)
    chosen = routes_ref[...]
    wtab[e] = jnp.concatenate(
        [jnp.sum(jnp.where(chosen == j, weight, 0.0), axis=0, keepdims=True) for j in range(E)],
        axis=0,
    )
    with jax.named_scope("barrier"):
        pl.semaphore_wait(barrier, E - 1 + T - 1)

    sent = []

    def send(cond, src, dst, recv, device):
        slot = len(sent)

        def build():
            return pltpu.make_async_remote_copy(
                src_ref=src, dst_ref=dst, send_sem=ssem.at[slot], recv_sem=recv,
                device_id=device, device_id_type=MESH,
            )

        sent.append((cond, build))
        if cond is None:
            build().start()
        else:
            @pl.when(cond)
            def _():
                build().start()

    def arrive(cond, dst, recv):
        def go():
            pltpu.make_async_remote_copy(
                src_ref=dst, dst_ref=dst, send_sem=ssem.at[0], recv_sem=recv,
                device_id=(e, mate), device_id_type=MESH,
            ).wait_recv()

        if cond is None:
            go()
        else:
            pl.when(cond)(go)

    def both(p, q):
        return q if p is None else (p if q is None else jnp.logical_and(p, q))

    def send_token_block(cond, j, up, down, across, own=False):
        src = dst = tokall.at[t, j]
        recv = tok_rs.at[j, t]
        if up:
            send(both(cond, a + 1 < A), src, dst, recv, (e + B, t))
        if down:
            send(both(cond, a > 0), src, dst, recv, (e - B, t))
        if across:
            send(cond, src, dst, recv, (across_x, t))
        if not own:
            send(cond, src, dst, recv, (e, across_y))
            send(cond, src, dst, recv, (e, mate))

    def y_forward(cond, j):
        arrive(cond, tokall.at[across_y, j], tok_rs.at[j, across_y])
        send(cond, tokall.at[across_y, j], tokall.at[across_y, j], tok_rs.at[j, across_y], (e, mate))

    late = []

    def token_step(s):
        pending = list(late)
        late.clear()
        if s < A:
            up_ok, down_ok = a - s >= 0, a + s < A
            ju, jd = e - s * B, e + s * B
            arrive(up_ok, tokall.at[t, ju], tok_rs.at[ju, t])
            send_token_block(up_ok, ju, True, False, True)
            arrive(down_ok, tokall.at[t, jd], tok_rs.at[jd, t])
            send_token_block(down_ok, jd, False, True, True)
            late.extend([(up_ok, ju), (down_ok, jd)])
        if s <= A:
            for sign in (1, -1) if s > 1 else (1,):
                oa = a - sign * (s - 1)
                ok = None if s == 1 else (oa >= 0 if sign == 1 else oa < A)
                j = oa * B + (1 - b)
                arrive(ok, tokall.at[t, j], tok_rs.at[j, t])
                send_token_block(ok, j, False, False, False)
                late.append((ok, j))
        for cond, j in pending:
            y_forward(cond, j)

    def send_kv_block(cond, j):
        src = dst = kvall.at[j]
        recv = kv_rs.at[j]
        send(both(cond, a + 1 < A), src, dst, recv, (e + B, t))
        send(both(cond, across_x > j), src, dst, recv, (across_x, t))

    def kv_step(s):
        ok, j = a - s >= 0, e - s * B
        arrive(ok, kvall.at[j], kv_rs.at[j])
        send_kv_block(ok, j)

    def attend(j, diag):
        nc = rows // lanes
        tiles = list(range(heads))
        base = j * rows

        def score(h):
            lhs = jnp.concatenate(
                [kvall[j, :rows], fa[pl.ds(pl.multiple_of(base, rows), rows)]], axis=1
            )
            s = lax.dot_general(
                lhs, qa[h], (((1,), (1,)), ((), ())), preferred_element_type=f32
            )
            if diag:
                kp = lax.broadcasted_iota(jnp.int32, s.shape, 0)
                qp = lax.broadcasted_iota(jnp.int32, s.shape, 1)
                s = jnp.where(kp <= qp, s, -jnp.inf)
            return s

        def soften(h, s):
            top = jnp.max(s, axis=0, keepdims=True)
            factor = None
            if not diag:
                old = m_sc[h]
                top = jnp.maximum(top, old)
                factor = jnp.exp(old - top)
            m_sc[h] = top
            return jnp.exp(s - top).astype(bf16), factor

        def gather(h, p, factor):
            g = h // group
            vt = jnp.concatenate(
                [
                    kvall[j, rows + n * lanes + g * HEAD : rows + n * lanes + (g + 1) * HEAD]
                    for n in range(nc)
                ],
                axis=1,
            )
            lhs = jnp.concatenate([vt, jnp.ones((16, rows), bf16)], axis=0)
            pv = jnp.dot(lhs, p, preferred_element_type=f32)
            if not diag:
                pv = acc_sc[h] * factor + pv
            acc_sc[h] = pv

        held, soft = {}, {}
        for i in range(len(tiles) + 2):
            if i < len(tiles):
                held[i] = score(tiles[i])
            if 0 <= i - 1 < len(tiles):
                soft[i - 1] = soften(tiles[i - 1], held.pop(i - 1))
            if 0 <= i - 2 < len(tiles):
                gather(tiles[i - 2], *soft.pop(i - 2))

    def attend_if(cond, j, wait):
        @pl.when(cond)
        def _():
            if wait:
                arrive(None, kvall.at[j], kv_rs.at[j])
            with jax.named_scope("att"):
                attend(j, False)

    def up(s):
        attend_if(a - s >= 0, e - s * B, False)

    def side(s):
        j = (a - s) * B + (1 - b)
        attend_if(jnp.logical_and(a - s >= 0, j < e), j, True)

    crows = B * erows

    def chunk_z(i):
        if A == 4:
            half = a // 2
            return [a + 1 - 2 * (a % 2), 2 - half, 3 - 3 * half, a][i]
        return lax.rem(a + i + 1, A)

    def expert_chunk(i):
        start = chunk_z(i) * B
        mine = i == A - 1
        scale = []
        for k in range(B):
            for oy in range(2):
                quarter = oy * 2 + (1 - c)
                arrive(
                    (start + k != e) if mine else None,
                    tokall.at[quarter, start + k], tok_rs.at[start + k, quarter],
                )
            arrive((start + k != e) if mine else None, wtab.at[start + k], wt_rs.at[start + k])
            columns = wtab[start + k].T
            lane = lax.broadcasted_iota(jnp.int32, columns.shape, 1)
            scale.append(jnp.sum(jnp.where(lane == e, columns, 0.0), axis=1, keepdims=True))
        scale = jnp.concatenate(scale, axis=0)
        x = jnp.concatenate(
            [tokall[qt, pl.ds(start, B)].reshape(crows, part) for qt in range(T)], axis=1
        )
        gate = jnp.dot(x, gw[...], preferred_element_type=f32)
        up_sum = jnp.dot(x, uw[...], preferred_element_type=f32)
        gate = jnp.minimum(gate, clamp_limit)
        up_sum = jnp.clip(up_sum, -clamp_limit, clamp_limit)
        hidden = ((up_sum + 1.0) * gate * jax.nn.sigmoid(sigmoid_slope * gate)).astype(bf16)

        def down(oy, oc):
            col = pl.multiple_of((oy * 2 + oc) * part, part)
            out = jnp.dot(hidden, dw[:, pl.ds(col, part)], preferred_element_type=f32)
            return (out * scale).astype(bf16).reshape(B, erows, part)

        for p, oy in enumerate((1 - y, y)):
            s1s[i, p] = down(oy, 1 - c)
            send(None, s1s.at[i, p], s1r.at[i, p], s1_rs.at[i, p], (e, mate))
        for p, oy in enumerate((1 - y, y)):
            s1o[i, p] = down(oy, c)

    def add(*terms):
        total = terms[0].astype(f32)
        for term in terms[1:]:
            total = total + term.astype(f32)
        return total.astype(bf16)

    def pair_step(i):
        arrive(None, s1r.at[i, 0], s1_rs.at[i, 0])
        s2s[i] = add(s1o[i, 0], s1r[i, 0])
        send(None, s2s.at[i], s2r.at[i], s2_rs.at[i], (e, across_y))

    def y_step(i):
        arrive(None, s1r.at[i, 1], s1_rs.at[i, 1])
        arrive(None, s2r.at[i], s2_rs.at[i])
        s3s[i] = add(s1o[i, 1, 1 - b], s1r[i, 1, 1 - b], s2r[i, 1 - b])
        send(None, s3s.at[i], s3r.at[i], s3_rs.at[i], (across_x, t))

    def x_step(i):
        arrive(None, s3r.at[i], s3_rs.at[i])
        out = add(s1o[i, 1, b], s1r[i, 1, b], s2r[i, b], s3r[i])
        if i == A - 1:
            zr[a] = out
        else:
            zs[i] = out
            send(None, zs.at[i], zr.at[a], z_rs.at[a], (chunk_z(i) * B + b, t))

    def scoped(name, f, *args):
        with jax.named_scope(name):
            f(*args)

    send_token_block(None, e, True, True, True, own=True)
    for d in range(1, E):
        j = lax.rem(e + d, E)
        send(None, wtab.at[e], wtab.at[e], wt_rs.at[e], (j, t))

    def prepare():
        zero = jnp.zeros((rows, HEAD), bf16)
        lane = lax.broadcasted_iota(jnp.int32, (rows, lanes), 1)
        for h in range(heads):
            q = q_ref[:, h * HEAD : (h + 1) * HEAD] * jnp.asarray(0.125, bf16)
            qa[h, :, :lanes] = jnp.concatenate([q, zero] if h < group else [zero, q], axis=1)
            chosen_lane = (lane == h) | (lane == h + 8) | (lane == h + 16)
            qa[h, :, lanes:] = jnp.where(chosen_lane, -1.0, 0.0).astype(bf16)
        kvall[e, :rows] = jnp.concatenate(
            [kv_ref[:, g * lanes : g * lanes + HEAD] for g in range(kv_heads)], axis=1
        )
        values = jnp.concatenate(
            [kv_ref[:, g * lanes + HEAD : (g + 1) * lanes] for g in range(kv_heads)], axis=1
        )
        for n in range(rows // lanes):
            kvall[e, rows + n * lanes : rows + (n + 1) * lanes] = values[
                n * lanes : (n + 1) * lanes
            ].T
        first = f_ref[:, pl.ds(pl.multiple_of(e * rows, rows), lanes)][:, :1]
        gates = f_ref[...] - first
        high = gates.astype(bf16).astype(f32)
        rest = gates - high
        middle = rest.astype(bf16).astype(f32)
        low = rest - middle
        blank = jnp.zeros((8 - heads, gates.shape[1]), f32)
        stack = jnp.concatenate(
            [high, blank, middle, blank, low, blank, jnp.zeros((lanes - 24, gates.shape[1]), f32)],
            axis=0,
        )
        for n in range(gates.shape[1] // lanes):
            fa[n * lanes : (n + 1) * lanes] = stack[:, n * lanes : (n + 1) * lanes].T.astype(bf16)

    scoped("prepare", prepare)
    scoped("tok1", token_step, 1)
    scoped("tok2", token_step, 2)
    send_kv_block(None, e)
    scoped("diag", attend, e, True)
    scoped("tok3", token_step, 3)
    for copy in weight_copies[:3]:
        copy.wait()

    scoped("chunk0", expert_chunk, 0)
    scoped("tok4", token_step, 4)
    scoped("kv1", kv_step, 1)
    scoped("pair0", pair_step, 0)
    scoped("chunk1", expert_chunk, 1)
    scoped("tok5", token_step, 5)
    scoped("pair1", pair_step, 1)
    up(1)
    scoped("y0", y_step, 0)
    scoped("chunk2", expert_chunk, 2)
    scoped("kv2", kv_step, 2)
    scoped("pair2", pair_step, 2)
    side(0)
    scoped("y1", y_step, 1)
    scoped("x0", x_step, 0)
    scoped("chunk3", expert_chunk, 3)
    scoped("pair3", pair_step, 3)
    up(2)
    side(1)
    scoped("kv3", kv_step, 3)
    scoped("y2", y_step, 2)
    scoped("x1", x_step, 1)
    up(3)
    side(2)
    scoped("y3", y_step, 3)
    scoped("x2", x_step, 2)
    side(3)

    def attention_out():
        arows = rows // T
        for h in range(heads):
            acc = acc_sc[h]
            out = (acc[:HEAD] / acc[HEAD : HEAD + 1]).T.astype(bf16)
            for tt in range(T):
                att[tt, :, h * HEAD : (h + 1) * HEAD] = out[tt * arows : (tt + 1) * arows]
        attall[t] = att[t]
        for d in range(1, T):
            ot = lax.rem(t + d, T)
            send(None, att.at[ot], attall.at[t], att_rs.at[t], (e, ot))

    scoped("attout", attention_out)
    scoped("x3", x_step, 3)
    weight_copies[3].wait()

    def mixer():
        for d in range(1, T):
            ot = lax.rem(t + d, T)
            arrive(None, attall.at[ot], att_rs.at[ot])
        mixed = jnp.concatenate([attall[tt] for tt in range(T)], axis=1).astype(f32)
        inverse = lax.rsqrt(jnp.mean(mixed * mixed, axis=-1, keepdims=True) + epsilon)
        mixed = (mixed * inverse * hg_ref[...]).astype(bf16)
        mix_ref[...] = jnp.dot(mixed, ow[...], preferred_element_type=f32).astype(bf16)

    scoped("mixer", mixer)

    def combine():
        for d in range(1, A):
            oz = lax.rem(a + d, A)
            arrive(None, zr.at[oz], z_rs.at[oz])
        moe_ref[...] = add(*[zr[oz] for oz in range(A)])

    scoped("combine", combine)

    for cond, build in sent:
        if cond is None:
            build().wait_send()
        else:
            @pl.when(cond)
            def _():
                build().wait_send()


def fused_body(*args):
    (queries, keys_values, forget_cache, heads_gain, output_weight, expert_tokens,
     expert_gain, routes, route_logits, gate_weight, up_weight, down_weight) = args
    E, T = lax.axis_size("ep"), lax.axis_size("tp")
    rows = queries.shape[0]
    heads = queries.shape[1] // HEAD
    erows, width = expert_tokens.shape
    part = width // T
    B = 2
    A = E // B
    bf16, f32 = jnp.bfloat16, jnp.float32
    V, DMA = pltpu.VMEM, pltpu.SemaphoreType.DMA
    vm = pl.BlockSpec(memory_space=pltpu.VMEM)
    hbm = pl.BlockSpec(memory_space=pltpu.HBM)

    operands = [
        queries, keys_values, forget_cache, heads_gain.reshape(1, -1), output_weight, expert_tokens,
        expert_gain.reshape(1, -1), routes.T, route_logits.T, gate_weight, up_weight, down_weight,
    ]
    small = [5, 6, 7, 8, 1, 0, 2, 3]

    def kernel(*refs):
        refs = list(refs)
        load_sem = refs.pop()
        held = refs[-len(small) :]
        refs = refs[: -len(small)]
        loads = []
        for n, (index, place) in enumerate(zip(small, held)):
            loads.append(pltpu.make_async_copy(refs[index], place, load_sem.at[n]))
            refs[index] = place
        fused_kernel(E, T, loads, *refs)

    return pl.pallas_call(
        kernel,
        out_shape=(
            jax.ShapeDtypeStruct((rows // T, output_weight.shape[1]), bf16),
            jax.ShapeDtypeStruct((erows, part), bf16),
        ),
        in_specs=[hbm] * len(operands),
        out_specs=(vm, vm),
        scratch_shapes=[
            V(output_weight.shape, bf16),
            V(gate_weight.shape[1:], bf16),
            V(up_weight.shape[1:], bf16),
            V(down_weight.shape[1:], bf16),
            V((T, E, erows, part), bf16),
            V((E, 2 * rows, 2 * HEAD), bf16),
            V((heads, rows, 4 * HEAD), bf16),
            V((E * rows, 2 * HEAD), bf16),
            V((heads, 1, rows), f32),
            V((heads, HEAD + 16, rows), f32),
            V((A, 2, B, erows, part), bf16),
            V((A, 2, B, erows, part), bf16),
            V((A, 2, B, erows, part), bf16),
            V((A, B, erows, part), bf16),
            V((A, B, erows, part), bf16),
            V((A, erows, part), bf16),
            V((A, erows, part), bf16),
            V((A, erows, part), bf16),
            V((A, erows, part), bf16),
            V((E, E, erows), f32),
            V((T, rows // T, queries.shape[1]), bf16),
            V((T, rows // T, queries.shape[1]), bf16),
            DMA((4,)),
            DMA((128,)),
            DMA((E, T)),
            DMA((E,)),
            DMA((A, 2)),
            DMA((A,)),
            DMA((A,)),
            DMA((A,)),
            DMA((E,)),
            DMA((T,)),
        ]
        + [V(operands[n].shape, operands[n].dtype) for n in small]
        + [DMA((len(small),))],
        compiler_params=pltpu.CompilerParams(
            collective_id=0, has_side_effects=True, vmem_limit_bytes=60 * 1024 * 1024
        ),
    )(*operands)


def pick_body(*args):
    queries, keys_values, routes = args[0], args[1], args[7]
    rows, picks = routes.shape
    E, T = lax.axis_size("ep"), lax.axis_size("tp")
    capacity = 2 * rows * picks // E
    shapes = queries.shape[1] == 4 * HEAD and keys_values.shape[1] == 4 * HEAD
    if capacity >= rows and T == 4 and E == 8 and shapes:
        return fused_body(*args)
    return body(*args)


def solution(mesh):
    placed = (
        P("ep", "tp"),
        P("ep", "tp"),
        P("tp", None),
        P(),
        P(),
        P("ep", None),
        P(),
        P("ep", None),
        P("ep", None),
        P("ep", None, "tp"),
        P("ep", None, "tp"),
        P("ep", "tp", None),
    )
    return jax.shard_map(
        pick_body,
        mesh=mesh,
        in_specs=placed,
        out_specs=(P(("ep", "tp"), None), P("ep", "tp")),
        check_vma=False,
    )
```

time: 87.5 us -> 73.5 us (0.84)
  the two profiles are of different devices: /device:TPU:10 before, /device:TPU:0 now
where the time goes in v1:
time: 73.5 us; the launch traced here: 73.2 us
  Pallas kernels  69.2 us (94%)
  local copies, waits for them, and re-layouts  3.45 us (5%)
    pallas_call x1, Pallas kernels, fused_body(): pl.pallas_call(kernel, out_shape=(jax.ShapeDtypeStruct((rows // T, output...  69.2 us
    unnamed x2, local copies, waits for them, and re-layouts  3.45 us

profile of v1, /device:TPU:0, one launch (start us, length us, event | category | flops | bytes accessed | tf_op | source)
XLA Modules:
  0.0 73.2 jit_solution(14568872397549679120)
XLA Ops:
  0.6 69.2 %shard_map.131 = (bf16[128,2048]{1,0:T(8,128)(2,1)}, bf16[128,512]{1,0:T(8,128)(2,1)}) custom-call(bf16[512,256]{1,0:T(8,128)(2,1)} %refs_0_.1, bf16[512,256]{1,0:T(8,128)(2,1)} %refs_1_.1, f32[4,4096]{1,0:T(4,128)} %refs_2_.1, f32[1,1024]{1,0:T(1,128)} %bitcast.5, bf16[1024,2048]{1,0:T(8,128)(2,1)} %refs_4_.1, bf16[128,2048]{1,0:T(8,128)(2,1)} %refs_5_.1, ...), custom_call_target="tpu_custom_call" | custom-call | tf_op jit(solution)/shard_map/pallas_call | solution.py:629
  69.8 1.9 %copy.16 = bf16[128,2048]{1,0:T(8,128)(2,1)} copy(bf16[128,2048]{1,0:T(8,128)(2,1)} %get-tuple-element.4) | data formatting | bytes 1048576
  71.7 1.6 %copy.17 = bf16[128,512]{1,0:T(8,128)(2,1)} copy(bf16[128,512]{1,0:T(8,128)(2,1)} %get-tuple-element.5) | data formatting | bytes 262144

commit v2 on v1

--- a/solution.py
+++ b/solution.py
@@ -184,6 +184,7 @@
 
 
 MESH = pl.DeviceIdType.MESH
+SEND_SLOTS = 96
 
 
 def fused_kernel(
@@ -191,9 +192,10 @@
     q_ref, kv_ref, f_ref, hg_ref, ow_hbm, tok_ref, eg_ref, routes_ref, logits_ref,
     gw_hbm, uw_hbm, dw_hbm,
     mix_ref, moe_ref,
-    ow, gw, uw, dw, tokall, kvall, qa, fa, m_sc, acc_sc,
+    ow, gw, uw, dw, tokall, qraw, kvraw, qx, kvx, kvall, qa, fa, m_sc, acc_sc,
     s1s, s1r, s1o, s2s, s2r, s3s, s3r, zs, zr, wtab, att, attall,
-    wsem, ssem, tok_rs, kv_rs, s1_rs, s2_rs, s3_rs, z_rs, wt_rs, att_rs,
+    wsem, ssem, tok_rs, top_rs, qx_rs, kvx_rs, kv_rs, s1_rs, s2_rs, s3_rs, z_rs, wt_rs,
+    att_rs,
 ):
     f32, bf16 = jnp.float32, jnp.bfloat16
     e = lax.axis_index("ep")
@@ -206,12 +208,17 @@
     across_y = (1 - y) * 2 + c
     across_x = a * B + (1 - b)
     rows = q_ref.shape[0]
-    heads = q_ref.shape[1] // HEAD
-    kv_heads = kv_ref.shape[1] // (2 * HEAD)
-    group = heads // kv_heads
+    heads = q_ref.shape[1] // HEAD // B
     erows, width = tok_ref.shape
     part = width // T
+    half = part // 2
     lanes = 2 * HEAD
+    extra = erows // 4
+    loads = loads + [
+        pltpu.make_async_copy(ref.at[:, g * lanes : (g + 1) * lanes], place.at[g], wsem.at[4 + 2 * n + g])
+        for n, (ref, place) in enumerate(((kv_ref, kvraw), (q_ref, qraw)))
+        for g in range(B)
+    ]
 
     weight_copies = [
         pltpu.make_async_copy(gw_hbm.at[0], gw, wsem.at[0]),
@@ -226,7 +233,9 @@
     for d in range(1, E):
         pl.semaphore_signal(barrier, inc=1, device_id=(lax.rem(e + d, E), t), device_id_type=MESH)
     for d in range(1, T):
-        pl.semaphore_signal(barrier, inc=1, device_id=(e, lax.rem(t + d, T)), device_id_type=MESH)
+        ot = lax.rem(t + d, T)
+        pl.semaphore_signal(barrier, inc=1, device_id=(e, ot), device_id_type=MESH)
+        pl.semaphore_signal(barrier, inc=1, device_id=(across_x, ot), device_id_type=MESH)
 
     for copy in loads:
         copy.wait()
@@ -247,12 +256,12 @@
         axis=0,
     )
     with jax.named_scope("barrier"):
-        pl.semaphore_wait(barrier, E - 1 + T - 1)
-
-    sent = []
+        pl.semaphore_wait(barrier, E - 1 + 2 * (T - 1))
+
+    sent, free = [], list(range(SEND_SLOTS))
 
     def send(cond, src, dst, recv, device):
-        slot = len(sent)
+        slot = free.pop(0)
 
         def build():
             return pltpu.make_async_remote_copy(
@@ -260,7 +269,7 @@
                 device_id=device, device_id_type=MESH,
             )
 
-        sent.append((cond, build))
+        sent.append((slot, cond, build))
         if cond is None:
             build().start()
         else:
@@ -268,6 +277,18 @@
             def _():
                 build().start()
 
+    def retire(entries):
+        for entry in list(entries):
+            slot, cond, build = entry
+            if cond is None:
+                build().wait_send()
+            else:
+                @pl.when(cond)
+                def _():
+                    build().wait_send()
+            sent.remove(entry)
+            free.append(slot)
+
     def arrive(cond, dst, recv):
         def go():
             pltpu.make_async_remote_copy(
@@ -284,21 +305,31 @@
         return q if p is None else (p if q is None else jnp.logical_and(p, q))
 
     def send_token_block(cond, j, up, down, across, own=False):
-        src = dst = tokall.at[t, j]
-        recv = tok_rs.at[j, t]
-        if up:
-            send(both(cond, a + 1 < A), src, dst, recv, (e + B, t))
-        if down:
-            send(both(cond, a > 0), src, dst, recv, (e - B, t))
-        if across:
-            send(cond, src, dst, recv, (across_x, t))
+        pieces = [(tokall.at[t, j], tok_rs.at[j, t])]
+        if not (up is False and down is False and across is False):
+            pieces.append((tokall.at[across_y, j, :extra], top_rs.at[j]))
+        for ref, recv in pieces:
+            for go, inside, to in (
+                (up, a + 1 < A, (e + B, t)),
+                (down, a > 0, (e - B, t)),
+                (across, None, (across_x, t)),
+            ):
+                if go is not False:
+                    send(both(cond, both(None if go is True else go, inside)), ref, ref, recv, to)
         if not own:
-            send(cond, src, dst, recv, (e, across_y))
-            send(cond, src, dst, recv, (e, mate))
+            ref = tokall.at[t, j, extra:]
+            send(cond, ref, ref, tok_rs.at[j, t], (e, across_y))
+            ref = tokall.at[t, j]
+            send(cond, ref, ref, tok_rs.at[j, t], (e, mate))
+
+    def arrive_token(cond, j):
+        arrive(cond, tokall.at[t, j], tok_rs.at[j, t])
+        arrive(cond, tokall.at[across_y, j, :extra], top_rs.at[j])
 
     def y_forward(cond, j):
-        arrive(cond, tokall.at[across_y, j], tok_rs.at[j, across_y])
-        send(cond, tokall.at[across_y, j], tokall.at[across_y, j], tok_rs.at[j, across_y], (e, mate))
+        arrive(cond, tokall.at[across_y, j, extra:], tok_rs.at[j, across_y])
+        ref = tokall.at[across_y, j]
+        send(cond, ref, ref, tok_rs.at[j, across_y], (e, mate))
 
     late = []
 
@@ -308,106 +339,150 @@
         if s < A:
             up_ok, down_ok = a - s >= 0, a + s < A
             ju, jd = e - s * B, e + s * B
-            arrive(up_ok, tokall.at[t, ju], tok_rs.at[ju, t])
-            send_token_block(up_ok, ju, True, False, True)
-            arrive(down_ok, tokall.at[t, jd], tok_rs.at[jd, t])
-            send_token_block(down_ok, jd, False, True, True)
+            arrive_token(up_ok, ju)
+            send_token_block(up_ok, ju, True, False, a - s > 0)
+            arrive_token(down_ok, jd)
+            send_token_block(down_ok, jd, False, True, a + s < A - 1)
             late.extend([(up_ok, ju), (down_ok, jd)])
         if s <= A:
-            for sign in (1, -1) if s > 1 else (1,):
+            for sign in (1, -1) if s > 1 else (0,):
                 oa = a - sign * (s - 1)
                 ok = None if s == 1 else (oa >= 0 if sign == 1 else oa < A)
                 j = oa * B + (1 - b)
-                arrive(ok, tokall.at[t, j], tok_rs.at[j, t])
-                send_token_block(ok, j, False, False, False)
+                arrive_token(ok, j)
+                rise = oa == 0 if sign >= 0 else False
+                fall = oa == A - 1 if sign <= 0 else False
+                send_token_block(ok, j, rise, fall, False)
                 late.append((ok, j))
         for cond, j in pending:
             y_forward(cond, j)
 
-    def send_kv_block(cond, j):
-        src = dst = kvall.at[j]
-        recv = kv_rs.at[j]
-        send(both(cond, a + 1 < A), src, dst, recv, (e + B, t))
-        send(both(cond, across_x > j), src, dst, recv, (across_x, t))
+    def swap_kv():
+        send(None, kvraw.at[1 - b], kvx, kvx_rs.at[0], (across_x, t))
+
+    def swap_q():
+        send(None, qraw.at[1 - b], qx, qx_rs.at[0], (across_x, t))
+
+    def send_kv_row(cond, row):
+        send(both(cond, a + 1 < A), kvall.at[row], kvall.at[row], kv_rs.at[row], (e + B, t))
 
     def kv_step(s):
-        ok, j = a - s >= 0, e - s * B
-        arrive(ok, kvall.at[j], kv_rs.at[j])
-        send_kv_block(ok, j)
-
-    def attend(j, diag):
+        ok, row = a - s >= 0, a - s
+        arrive(ok, kvall.at[row], kv_rs.at[row])
+        send_kv_row(ok, row)
+
+    def by_block(mine, other):
+        return [jnp.where(b == 0, mine, other), jnp.where(b == 0, other, mine)]
+
+    def pack_kv():
+        arrive(None, kvx, kvx_rs.at[0])
+        blocks = by_block(kvraw[b], kvx[...])
+        kvall[a, :rows] = jnp.concatenate([block[:, :HEAD] for block in blocks], axis=1)
+        values = jnp.concatenate([block[:, HEAD:] for block in blocks], axis=1)
+        for n in range(rows // lanes):
+            kvall[a, rows + n * lanes : rows + (n + 1) * lanes] = values[
+                n * lanes : (n + 1) * lanes
+            ].T
+        send_kv_row(None, a)
+
+    def pack_q():
+        arrive(None, qx, qx_rs.at[0])
+        zero = jnp.zeros((rows, HEAD), bf16)
+        lane = lax.broadcasted_iota(jnp.int32, (rows, lanes), 1)
+        for xb, block in enumerate(by_block(qraw[b], qx[...])):
+            block = block * jnp.asarray(0.125, bf16)
+            for h in range(heads):
+                q = block[:, h * HEAD : (h + 1) * HEAD]
+                chosen_lane = (lane == h) | (lane == h + 8) | (lane == h + 16)
+                pick = jnp.where(chosen_lane, -1.0, 0.0).astype(bf16)
+                for kb in range(B):
+                    qa[h, xb, kb, :, :lanes] = jnp.concatenate(
+                        [q, zero] if kb == 0 else [zero, q], axis=1
+                    )
+                    qa[h, xb, kb, :, lanes:] = pick
+
+    def pack_gates():
+        count = f_ref.shape[1]
+        gates = f_ref[...]
+        gates = jnp.where(b == 0, gates[:heads], gates[heads:])
+        first = f_ref[:, pl.ds(pl.multiple_of(a * B * rows, rows), lanes)][:, :1]
+        gates = gates - jnp.where(b == 0, first[:heads], first[heads:])
+        high = gates.astype(bf16).astype(f32)
+        rest = gates - high
+        middle = rest.astype(bf16).astype(f32)
+        low = rest - middle
+        blank = jnp.zeros((8 - heads, count), f32)
+        stack = jnp.concatenate(
+            [high, blank, middle, blank, low, blank, jnp.zeros((lanes - 24, count), f32)], axis=0
+        )
+        for n in range(count // lanes):
+            fa[n * lanes : (n + 1) * lanes] = stack[:, n * lanes : (n + 1) * lanes].T.astype(bf16)
+
+    def attend(row, tiles):
         nc = rows // lanes
-        tiles = list(range(heads))
-        base = j * rows
-
-        def score(h):
-            lhs = jnp.concatenate(
-                [kvall[j, :rows], fa[pl.ds(pl.multiple_of(base, rows), rows)]], axis=1
+
+        def score(h, xb, kb, start):
+            gate = fa[pl.ds(pl.multiple_of((row * B + kb) * rows, rows), rows)]
+            lhs = jnp.concatenate([kvall[row, :rows], gate], axis=1)
+            s = lax.dot_general(
+                lhs, qa[h, xb, kb], (((1,), (1,)), ((), ())), preferred_element_type=f32
             )
-            s = lax.dot_general(
-                lhs, qa[h], (((1,), (1,)), ((), ())), preferred_element_type=f32
-            )
-            if diag:
+            if start is not None and xb == kb:
                 kp = lax.broadcasted_iota(jnp.int32, s.shape, 0)
                 qp = lax.broadcasted_iota(jnp.int32, s.shape, 1)
                 s = jnp.where(kp <= qp, s, -jnp.inf)
             return s
 
-        def soften(h, s):
+        def soften(h, xb, kb, start, s):
             top = jnp.max(s, axis=0, keepdims=True)
             factor = None
-            if not diag:
-                old = m_sc[h]
+            if not start:
+                old = m_sc[h, xb]
                 top = jnp.maximum(top, old)
                 factor = jnp.exp(old - top)
-            m_sc[h] = top
+            m_sc[h, xb] = top
             return jnp.exp(s - top).astype(bf16), factor
 
-        def gather(h, p, factor):
-            g = h // group
+        def gather(h, xb, kb, start, p, factor):
             vt = jnp.concatenate(
                 [
-                    kvall[j, rows + n * lanes + g * HEAD : rows + n * lanes + (g + 1) * HEAD]
+                    kvall[row, rows + n * lanes + kb * HEAD : rows + n * lanes + (kb + 1) * HEAD]
                     for n in range(nc)
                 ],
                 axis=1,
             )
             lhs = jnp.concatenate([vt, jnp.ones((16, rows), bf16)], axis=0)
             pv = jnp.dot(lhs, p, preferred_element_type=f32)
-            if not diag:
-                pv = acc_sc[h] * factor + pv
-            acc_sc[h] = pv
+            if not start:
+                pv = acc_sc[h, xb] * factor + pv
+            acc_sc[h, xb] = pv
 
         held, soft = {}, {}
         for i in range(len(tiles) + 2):
             if i < len(tiles):
-                held[i] = score(tiles[i])
+                held[i] = score(*tiles[i])
             if 0 <= i - 1 < len(tiles):
-                soft[i - 1] = soften(tiles[i - 1], held.pop(i - 1))
+                soft[i - 1] = soften(*tiles[i - 1], held.pop(i - 1))
             if 0 <= i - 2 < len(tiles):
-                gather(tiles[i - 2], *soft.pop(i - 2))
-
-    def attend_if(cond, j, wait):
-        @pl.when(cond)
+                gather(*tiles[i - 2], *soft.pop(i - 2))
+
+    def attend_own():
+        tiles = [(h, xb, xb, True) for xb in range(B) for h in range(heads)]
+        tiles += [(h, xb, kb, False) for xb in range(B) for kb in range(xb) for h in range(heads)]
+        own = [(h, xb, kb, start) for h, xb, kb, start in tiles]
+        attend(a, own)
+
+    def up(s, xb):
+        @pl.when(a - s >= 0)
         def _():
-            if wait:
-                arrive(None, kvall.at[j], kv_rs.at[j])
             with jax.named_scope("att"):
-                attend(j, False)
-
-    def up(s):
-        attend_if(a - s >= 0, e - s * B, False)
-
-    def side(s):
-        j = (a - s) * B + (1 - b)
-        attend_if(jnp.logical_and(a - s >= 0, j < e), j, True)
+                attend(a - s, [(h, xb, kb, None) for kb in range(B) for h in range(heads)])
 
     crows = B * erows
 
     def chunk_z(i):
         if A == 4:
-            half = a // 2
-            return [a + 1 - 2 * (a % 2), 2 - half, 3 - 3 * half, a][i]
+            return [a + 1 - 2 * (a % 2), 2 - a // 2, 3 - 3 * (a // 2), a][i]
         return lax.rem(a + i + 1, A)
 
     def expert_chunk(i):
@@ -435,16 +510,19 @@
         up_sum = jnp.clip(up_sum, -clamp_limit, clamp_limit)
         hidden = ((up_sum + 1.0) * gate * jax.nn.sigmoid(sigmoid_slope * gate)).astype(bf16)
 
-        def down(oy, oc):
+        def down(oy, oc, place):
             col = pl.multiple_of((oy * 2 + oc) * part, part)
             out = jnp.dot(hidden, dw[:, pl.ds(col, part)], preferred_element_type=f32)
-            return (out * scale).astype(bf16).reshape(B, erows, part)
+            out = (out * scale).astype(bf16)
+            for n in range(2):
+                place[n] = out[:, n * half : (n + 1) * half].reshape(B, erows, half)
 
         for p, oy in enumerate((1 - y, y)):
-            s1s[i, p] = down(oy, 1 - c)
-            send(None, s1s.at[i, p], s1r.at[i, p], s1_rs.at[i, p], (e, mate))
+            down(oy, 1 - c, s1s.at[i, :, p])
+        for n in range(2):
+            send(None, s1s.at[i, n], s1r.at[i, n], s1_rs.at[i, n], (e, mate))
         for p, oy in enumerate((1 - y, y)):
-            s1o[i, p] = down(oy, c)
+            down(oy, c, s1o.at[i, :, p])
 
     def add(*terms):
         total = terms[0].astype(f32)
@@ -452,24 +530,30 @@
             total = total + term.astype(f32)
         return total.astype(bf16)
 
-    def pair_step(i):
+    def first_step(i):
         arrive(None, s1r.at[i, 0], s1_rs.at[i, 0])
-        s2s[i] = add(s1o[i, 0], s1r[i, 0])
-        send(None, s2s.at[i], s2r.at[i], s2_rs.at[i], (e, across_y))
-
-    def y_step(i):
+        s2s[i, 0] = add(s1o[i, 0, 0], s1r[i, 0, 0])
+        send(None, s2s.at[i, 0], s2r.at[i, 0], s2_rs.at[i, 0], (e, across_y))
         arrive(None, s1r.at[i, 1], s1_rs.at[i, 1])
-        arrive(None, s2r.at[i], s2_rs.at[i])
-        s3s[i] = add(s1o[i, 1, 1 - b], s1r[i, 1, 1 - b], s2r[i, 1 - b])
-        send(None, s3s.at[i], s3r.at[i], s3_rs.at[i], (across_x, t))
-
-    def x_step(i):
-        arrive(None, s3r.at[i], s3_rs.at[i])
-        out = add(s1o[i, 1, b], s1r[i, 1, b], s2r[i, b], s3r[i])
-        if i == A - 1:
-            zr[a] = out
-        else:
-            zs[i] = out
+        for p in range(2):
+            s2s[i, 1, p] = add(s1o[i, 1, p, 1 - b], s1r[i, 1, p, 1 - b])
+        send(None, s2s.at[i, 1], s2r.at[i, 1], s2_rs.at[i, 1], (across_x, t))
+
+    def second_step(i):
+        arrive(None, s2r.at[i, 0], s2_rs.at[i, 0])
+        s3s[i, 0] = add(s1o[i, 0, 1, 1 - b], s1r[i, 0, 1, 1 - b], s2r[i, 0, 1 - b])
+        send(None, s3s.at[i, 0], s3r.at[i, 0], s3_rs.at[i, 0], (across_x, t))
+        arrive(None, s2r.at[i, 1], s2_rs.at[i, 1])
+        s3s[i, 1] = add(s1o[i, 1, 0, b], s1r[i, 1, 0, b], s2r[i, 1, 0])
+        send(None, s3s.at[i, 1], s3r.at[i, 1], s3_rs.at[i, 1], (e, across_y))
+
+    def third_step(i):
+        place = zr.at[a] if i == A - 1 else zs.at[i]
+        arrive(None, s3r.at[i, 0], s3_rs.at[i, 0])
+        place[0] = add(s1o[i, 0, 1, b], s1r[i, 0, 1, b], s2r[i, 0, b], s3r[i, 0])
+        arrive(None, s3r.at[i, 1], s3_rs.at[i, 1])
+        place[1] = add(s1o[i, 1, 1, b], s1r[i, 1, 1, b], s2r[i, 1, 1], s3r[i, 1])
+        if i != A - 1:
             send(None, zs.at[i], zr.at[a], z_rs.at[a], (chunk_z(i) * B + b, t))
 
     def scoped(name, f, *args):
@@ -481,96 +565,80 @@
         j = lax.rem(e + d, E)
         send(None, wtab.at[e], wtab.at[e], wt_rs.at[e], (j, t))
 
-    def prepare():
-        zero = jnp.zeros((rows, HEAD), bf16)
-        lane = lax.broadcasted_iota(jnp.int32, (rows, lanes), 1)
-        for h in range(heads):
-            q = q_ref[:, h * HEAD : (h + 1) * HEAD] * jnp.asarray(0.125, bf16)
-            qa[h, :, :lanes] = jnp.concatenate([q, zero] if h < group else [zero, q], axis=1)
-            chosen_lane = (lane == h) | (lane == h + 8) | (lane == h + 16)
-            qa[h, :, lanes:] = jnp.where(chosen_lane, -1.0, 0.0).astype(bf16)
-        kvall[e, :rows] = jnp.concatenate(
-            [kv_ref[:, g * lanes : g * lanes + HEAD] for g in range(kv_heads)], axis=1
-        )
-        values = jnp.concatenate(
-            [kv_ref[:, g * lanes + HEAD : (g + 1) * lanes] for g in range(kv_heads)], axis=1
-        )
-        for n in range(rows // lanes):
-            kvall[e, rows + n * lanes : rows + (n + 1) * lanes] = values[
-                n * lanes : (n + 1) * lanes
-            ].T
-        first = f_ref[:, pl.ds(pl.multiple_of(e * rows, rows), lanes)][:, :1]
-        gates = f_ref[...] - first
-        high = gates.astype(bf16).astype(f32)
-        rest = gates - high
-        middle = rest.astype(bf16).astype(f32)
-        low = rest - middle
-        blank = jnp.zeros((8 - heads, gates.shape[1]), f32)
-        stack = jnp.concatenate(
-            [high, blank, middle, blank, low, blank, jnp.zeros((lanes - 24, gates.shape[1]), f32)],
-            axis=0,
-        )
-        for n in range(gates.shape[1] // lanes):
-            fa[n * lanes : (n + 1) * lanes] = stack[:, n * lanes : (n + 1) * lanes].T.astype(bf16)
-
-    scoped("prepare", prepare)
+    swap_kv()
+    scoped("gates", pack_gates)
     scoped("tok1", token_step, 1)
+    swap_q()
     scoped("tok2", token_step, 2)
-    send_kv_block(None, e)
-    scoped("diag", attend, e, True)
+    scoped("packkv", pack_kv)
+    scoped("packq", pack_q)
+    scoped("own", attend_own)
     scoped("tok3", token_step, 3)
     for copy in weight_copies[:3]:
         copy.wait()
-
+    retire(sent[:33])
     scoped("chunk0", expert_chunk, 0)
     scoped("tok4", token_step, 4)
     scoped("kv1", kv_step, 1)
-    scoped("pair0", pair_step, 0)
+    up(1, 0)
+    scoped("r1_0", first_step, 0)
+    scoped("tok5", token_step, 5)
     scoped("chunk1", expert_chunk, 1)
-    scoped("tok5", token_step, 5)
-    scoped("pair1", pair_step, 1)
-    up(1)
-    scoped("y0", y_step, 0)
+    up(1, 1)
+    scoped("r1_1", first_step, 1)
+    retire(sent[:44])
+    scoped("kv2", kv_step, 2)
+    scoped("r2_0", second_step, 0)
     scoped("chunk2", expert_chunk, 2)
-    scoped("kv2", kv_step, 2)
-    scoped("pair2", pair_step, 2)
-    side(0)
-    scoped("y1", y_step, 1)
-    scoped("x0", x_step, 0)
+    up(2, 0)
+    scoped("r1_2", first_step, 2)
+    scoped("r2_1", second_step, 1)
+    scoped("r3_0", third_step, 0)
     scoped("chunk3", expert_chunk, 3)
-    scoped("pair3", pair_step, 3)
-    up(2)
-    side(1)
     scoped("kv3", kv_step, 3)
-    scoped("y2", y_step, 2)
-    scoped("x1", x_step, 1)
-    up(3)
-    side(2)
-    scoped("y3", y_step, 3)
-    scoped("x2", x_step, 2)
-    side(3)
-
-    def attention_out():
-        arows = rows // T
-        for h in range(heads):
-            acc = acc_sc[h]
-            out = (acc[:HEAD] / acc[HEAD : HEAD + 1]).T.astype(bf16)
-            for tt in range(T):
-                att[tt, :, h * HEAD : (h + 1) * HEAD] = out[tt * arows : (tt + 1) * arows]
-        attall[t] = att[t]
-        for d in range(1, T):
+    up(2, 1)
+    scoped("r1_3", first_step, 3)
+    scoped("r2_2", second_step, 2)
+    scoped("r3_1", third_step, 1)
+
+    arows = rows // T
+
+    def attention_out(xb):
+        out = jnp.concatenate(
+            [acc_sc[h, xb, :HEAD] / acc_sc[h, xb, HEAD : HEAD + 1] for h in range(heads)], axis=0
+        ).T.astype(bf16)
+        for tt in range(T):
+            att[xb, tt] = out[tt * arows : (tt + 1) * arows]
+
+        @pl.when(b == xb)
+        def _():
+            attall[t, b] = att[xb, t]
+
+        for d in range(T):
             ot = lax.rem(t + d, T)
-            send(None, att.at[ot], attall.at[t], att_rs.at[t], (e, ot))
-
-    scoped("attout", attention_out)
-    scoped("x3", x_step, 3)
+            send(
+                None if d else b != xb,
+                att.at[xb, ot], attall.at[t, b], att_rs.at[t, b], (a * B + xb, ot),
+            )
+
+    up(3, 0)
+    scoped("attout0", attention_out, 0)
+    up(3, 1)
+    scoped("attout1", attention_out, 1)
+    scoped("r2_3", second_step, 3)
+    scoped("r3_2", third_step, 2)
+    scoped("r3_3", third_step, 3)
     weight_copies[3].wait()
 
     def mixer():
-        for d in range(1, T):
-            ot = lax.rem(t + d, T)
-            arrive(None, attall.at[ot], att_rs.at[ot])
-        mixed = jnp.concatenate([attall[tt] for tt in range(T)], axis=1).astype(f32)
+        for dx in range(B):
+            for d in range(T):
+                if dx or d:
+                    ob, ot = lax.rem(b + dx, B), lax.rem(t + d, T)
+                    arrive(None, attall.at[ot, ob], att_rs.at[ot, ob])
+        mixed = jnp.concatenate(
+            [attall[tt, bb] for tt in range(T) for bb in range(B)], axis=1
+        ).astype(f32)
         inverse = lax.rsqrt(jnp.mean(mixed * mixed, axis=-1, keepdims=True) + epsilon)
         mixed = (mixed * inverse * hg_ref[...]).astype(bf16)
         mix_ref[...] = jnp.dot(mixed, ow[...], preferred_element_type=f32).astype(bf16)
@@ -581,17 +649,13 @@
         for d in range(1, A):
             oz = lax.rem(a + d, A)
             arrive(None, zr.at[oz], z_rs.at[oz])
-        moe_ref[...] = add(*[zr[oz] for oz in range(A)])
+        for n in range(2):
+            moe_ref[:, n * half : (n + 1) * half] = add(*[zr[oz, n] for oz in range(A)])
 
     scoped("combine", combine)
 
-    for cond, build in sent:
-        if cond is None:
-            build().wait_send()
-        else:
-            @pl.when(cond)
-            def _():
-                build().wait_send()
+    with jax.named_scope("drain"):
+        retire(sent)
 
 
 def fused_body(*args):
@@ -613,7 +677,9 @@
         queries, keys_values, forget_cache, heads_gain.reshape(1, -1), output_weight, expert_tokens,
         expert_gain.reshape(1, -1), routes.T, route_logits.T, gate_weight, up_weight, down_weight,
     ]
-    small = [5, 6, 7, 8, 1, 0, 2, 3]
+    small = [5, 6, 7, 8, 2, 3]
+    lanes, half = 2 * HEAD, part // 2
+    heads = heads // B
 
     def kernel(*refs):
         refs = list(refs)
@@ -628,10 +694,7 @@
 
     return pl.pallas_call(
         kernel,
-        out_shape=(
-            jax.ShapeDtypeStruct((rows // T, output_weight.shape[1]), bf16),
-            jax.ShapeDtypeStruct((erows, part), bf16),
-        ),
+        out_shape=(V((rows // T, output_weight.shape[1]), bf16), V((erows, part), bf16)),
         in_specs=[hbm] * len(operands),
         out_specs=(vm, vm),
         scratch_shapes=[
@@ -640,33 +703,40 @@
             V(up_weight.shape[1:], bf16),
             V(down_weight.shape[1:], bf16),
             V((T, E, erows, part), bf16),
-            V((E, 2 * rows, 2 * HEAD), bf16),
-            V((heads, rows, 4 * HEAD), bf16),
-            V((E * rows, 2 * HEAD), bf16),
-            V((heads, 1, rows), f32),
-            V((heads, HEAD + 16, rows), f32),
-            V((A, 2, B, erows, part), bf16),
-            V((A, 2, B, erows, part), bf16),
-            V((A, 2, B, erows, part), bf16),
-            V((A, B, erows, part), bf16),
-            V((A, B, erows, part), bf16),
-            V((A, erows, part), bf16),
-            V((A, erows, part), bf16),
-            V((A, erows, part), bf16),
-            V((A, erows, part), bf16),
+            V((B, rows, lanes), bf16),
+            V((B, rows, lanes), bf16),
+            V((rows, lanes), bf16),
+            V((rows, lanes), bf16),
+            V((A, 2 * rows, lanes), bf16),
+            V((heads, B, B, rows, 2 * lanes), bf16),
+            V((E * rows, lanes), bf16),
+            V((heads, B, 1, rows), f32),
+            V((heads, B, HEAD + 16, rows), f32),
+            V((A, 2, 2, B, erows, half), bf16),
+            V((A, 2, 2, B, erows, half), bf16),
+            V((A, 2, 2, B, erows, half), bf16),
+            V((A, 2, 2, erows, half), bf16),
+            V((A, 2, 2, erows, half), bf16),
+            V((A, 2, erows, half), bf16),
+            V((A, 2, erows, half), bf16),
+            V((A, 2, erows, half), bf16),
+            V((A, 2, erows, half), bf16),
             V((E, E, erows), f32),
-            V((T, rows // T, queries.shape[1]), bf16),
-            V((T, rows // T, queries.shape[1]), bf16),
-            DMA((4,)),
-            DMA((128,)),
+            V((B, T, rows // T, lanes), bf16),
+            V((T, B, rows // T, lanes), bf16),
+            DMA((8,)),
+            DMA((SEND_SLOTS,)),
             DMA((E, T)),
             DMA((E,)),
+            DMA((1,)),
+            DMA((1,)),
+            DMA((A,)),
+            DMA((A, 2)),
+            DMA((A, 2)),
             DMA((A, 2)),
             DMA((A,)),
-            DMA((A,)),
-            DMA((A,)),
             DMA((E,)),
-            DMA((T,)),
+            DMA((T, B)),
         ]
         + [V(operands[n].shape, operands[n].dtype) for n in small]
         + [DMA((len(small),))],

time: 73.5 us -> 63.7 us (0.87)
  Pallas kernels: 69.2 us -> 61.5 us
  local copies, waits for them, and re-layouts: 3.45 us -> 1.45 us
    pallas_call x1, Pallas kernels: 69.2 us -> 61.5 us  [fused_body(): pl.pallas_call(kernel, out_shape=(V((rows // T, output_weight.shape[1]),...]
    unnamed x2, local copies, waits for them, and re-layouts: 3.45 us -> 1.45 us
where the time goes in v2:
time: 63.7 us; the launch traced here: 63.6 us
  Pallas kernels  61.5 us (97%)
  local copies, waits for them, and re-layouts  1.45 us (2%)
  between operations  0.64 us (1%)
    pallas_call x1, Pallas kernels, fused_body(): pl.pallas_call(kernel, out_shape=(V((rows // T, output_weight.shape[1]),...  61.5 us
    unnamed x2, local copies, waits for them, and re-layouts  1.45 us

profile of v2, /device:TPU:0, one launch (start us, length us, event | category | flops | bytes accessed | tf_op | source)
XLA Modules:
  0.0 63.6 jit_solution(8077369342683070428)
XLA Ops:
  0.6 61.5 %shard_map.131 = (bf16[128,2048]{1,0:T(8,128)(2,1)S(1)}, bf16[128,512]{1,0:T(8,128)(2,1)S(1)}) custom-call(bf16[512,256]{1,0:T(8,128)(2,1)} %refs_0_.1, bf16[512,256]{1,0:T(8,128)(2,1)} %refs_1_.1, f32[4,4096]{1,0:T(4,128)} %refs_2_.1, f32[1,1024]{1,0:T(1,128)} %bitcast.5, bf16[1024,2048]{1,0:T(8,128)(2,1)} %refs_4_.1, bf16[128,2048]{1,0:T(8,128)(2,1)} %refs_5_.1, ...), custom_call_target="tpu_custom_call" | custom-call | tf_op jit(solution)/shard_map/pallas_call | solution.py:695
  62.2 0.8 %copy.16 = bf16[128,2048]{1,0:T(8,128)(2,1)} copy(bf16[128,2048]{1,0:T(8,128)(2,1)S(1)} %get-tuple-element.2) | data formatting | bytes 1048576
  63.0 0.7 %copy.17 = bf16[128,512]{1,0:T(8,128)(2,1)} copy(bf16[128,512]{1,0:T(8,128)(2,1)S(1)} %get-tuple-element.3) | data formatting | bytes 262144

commit v3 on v2

--- a/solution.py
+++ b/solution.py
@@ -184,7 +184,7 @@
 
 
 MESH = pl.DeviceIdType.MESH
-SEND_SLOTS = 96
+SEND_SLOTS = 88
 
 
 def fused_kernel(
@@ -237,10 +237,8 @@
         pl.semaphore_signal(barrier, inc=1, device_id=(e, ot), device_id_type=MESH)
         pl.semaphore_signal(barrier, inc=1, device_id=(across_x, ot), device_id_type=MESH)
 
-    for copy in loads:
+    for copy in loads[:4]:
         copy.wait()
-    for copy in weight_copies:
-        copy.start()
 
     tokens = tok_ref[...].astype(f32)
     inverse = lax.rsqrt(jnp.mean(tokens * tokens, axis=-1, keepdims=True) + epsilon)
@@ -482,7 +480,7 @@
 
     def chunk_z(i):
         if A == 4:
-            return [a + 1 - 2 * (a % 2), 2 - a // 2, 3 - 3 * (a // 2), a][i]
+            return [a + 1 - 2 * (a % 2), (a + 2) % 4, 3 - a, a][i]
         return lax.rem(a + i + 1, A)
 
     def expert_chunk(i):
@@ -561,9 +559,45 @@
             f(*args)
 
     send_token_block(None, e, True, True, True, own=True)
+    for copy in loads[4:]:
+        copy.wait()
+    for copy in weight_copies:
+        copy.start()
     for d in range(1, E):
         j = lax.rem(e + d, E)
         send(None, wtab.at[e], wtab.at[e], wt_rs.at[e], (j, t))
+
+    arows = rows // T
+
+    out_slots = [[free.pop(0) for _ in range(T)] for _ in range(B)]
+
+    def out_copy(xb, d):
+        ot = lax.rem(t + d, T)
+        return pltpu.make_async_remote_copy(
+            src_ref=att.at[xb, ot], dst_ref=attall.at[t, b], send_sem=ssem.at[out_slots[xb][d]],
+            recv_sem=att_rs.at[t, b], device_id=(a * B + xb, ot), device_id_type=MESH,
+        )
+
+    def attention_out(row, xb):
+        @pl.when(a == row)
+        def _():
+            with jax.named_scope("attout"):
+                out = jnp.concatenate(
+                    [acc_sc[h, xb, :HEAD] / acc_sc[h, xb, HEAD : HEAD + 1] for h in range(heads)],
+                    axis=0,
+                ).T.astype(bf16)
+                for tt in range(T):
+                    att[xb, tt] = out[tt * arows : (tt + 1) * arows]
+                for d in range(1, T):
+                    out_copy(xb, d).start()
+
+                @pl.when(b == xb)
+                def _():
+                    attall[t, b] = att[xb, t]
+
+                @pl.when(b != xb)
+                def _():
+                    out_copy(xb, 0).start()
 
     swap_kv()
     scoped("gates", pack_gates)
@@ -572,17 +606,20 @@
     scoped("tok2", token_step, 2)
     scoped("packkv", pack_kv)
     scoped("packq", pack_q)
+    retire(sent[:14])
     scoped("own", attend_own)
     scoped("tok3", token_step, 3)
     for copy in weight_copies[:3]:
         copy.wait()
-    retire(sent[:33])
+    retire(sent[:26])
     scoped("chunk0", expert_chunk, 0)
     scoped("tok4", token_step, 4)
     scoped("kv1", kv_step, 1)
     up(1, 0)
     scoped("r1_0", first_step, 0)
     scoped("tok5", token_step, 5)
+    attention_out(0, 0)
+    attention_out(0, 1)
     scoped("chunk1", expert_chunk, 1)
     up(1, 1)
     scoped("r1_1", first_step, 1)
@@ -592,41 +629,25 @@
     scoped("chunk2", expert_chunk, 2)
     up(2, 0)
     scoped("r1_2", first_step, 2)
+    attention_out(1, 0)
+    attention_out(1, 1)
+    scoped("chunk3", expert_chunk, 3)
     scoped("r2_1", second_step, 1)
-    scoped("r3_0", third_step, 0)
-    scoped("chunk3", expert_chunk, 3)
     scoped("kv3", kv_step, 3)
     up(2, 1)
     scoped("r1_3", first_step, 3)
+    scoped("r3_0", third_step, 0)
+    attention_out(2, 0)
+    attention_out(2, 1)
     scoped("r2_2", second_step, 2)
+
+    up(3, 0)
     scoped("r3_1", third_step, 1)
-
-    arows = rows // T
-
-    def attention_out(xb):
-        out = jnp.concatenate(
-            [acc_sc[h, xb, :HEAD] / acc_sc[h, xb, HEAD : HEAD + 1] for h in range(heads)], axis=0
-        ).T.astype(bf16)
-        for tt in range(T):
-            att[xb, tt] = out[tt * arows : (tt + 1) * arows]
-
-        @pl.when(b == xb)
-        def _():
-            attall[t, b] = att[xb, t]
-
-        for d in range(T):
-            ot = lax.rem(t + d, T)
-            send(
-                None if d else b != xb,
-                att.at[xb, ot], attall.at[t, b], att_rs.at[t, b], (a * B + xb, ot),
-            )
-
-    up(3, 0)
-    scoped("attout0", attention_out, 0)
     up(3, 1)
-    scoped("attout1", attention_out, 1)
     scoped("r2_3", second_step, 3)
     scoped("r3_2", third_step, 2)
+    attention_out(3, 0)
+    attention_out(3, 1)
     scoped("r3_3", third_step, 3)
     weight_copies[3].wait()
 
@@ -656,6 +677,13 @@
 
     with jax.named_scope("drain"):
         retire(sent)
+        for xb in range(B):
+            for d in range(1, T):
+                out_copy(xb, d).wait_send()
+
+            @pl.when(b != xb)
+            def _():
+                out_copy(xb, 0).wait_send()
 
 
 def fused_body(*args):

time: 63.7 us -> 62 us (0.973)
  Pallas kernels: 61.5 us -> 59.8 us
    pallas_call x1, Pallas kernels: 61.5 us -> 59.8 us  [fused_body(): pl.pallas_call(kernel, out_shape=(V((rows // T, output_weight.shape[1]),...]
where the time goes in v3:
time: 62 us; the launch traced here: 61.9 us
  Pallas kernels  59.8 us (96%)
  local copies, waits for them, and re-layouts  1.45 us (2%)
  between operations  0.64 us (1%)
    pallas_call x1, Pallas kernels, fused_body(): pl.pallas_call(kernel, out_shape=(V((rows // T, output_weight.shape[1]),...  59.8 us
    unnamed x2, local copies, waits for them, and re-layouts  1.45 us

profile of v3, /device:TPU:0, one launch (start us, length us, event | category | flops | bytes accessed | tf_op | source)
XLA Modules:
  0.0 61.9 jit_solution(10687966773842500953)
XLA Ops:
  0.6 59.8 %shard_map.131 = (bf16[128,2048]{1,0:T(8,128)(2,1)S(1)}, bf16[128,512]{1,0:T(8,128)(2,1)S(1)}) custom-call(bf16[512,256]{1,0:T(8,128)(2,1)} %refs_0_.1, bf16[512,256]{1,0:T(8,128)(2,1)} %refs_1_.1, f32[4,4096]{1,0:T(4,128)} %refs_2_.1, f32[1,1024]{1,0:T(1,128)} %bitcast.5, bf16[1024,2048]{1,0:T(8,128)(2,1)} %refs_4_.1, bf16[128,2048]{1,0:T(8,128)(2,1)} %refs_5_.1, ...), custom_call_target="tpu_custom_call" | custom-call | tf_op jit(solution)/shard_map/pallas_call | solution.py:723
  60.4 0.8 %copy.16 = bf16[128,2048]{1,0:T(8,128)(2,1)} copy(bf16[128,2048]{1,0:T(8,128)(2,1)S(1)} %get-tuple-element.2) | data formatting | bytes 1048576
  61.2 0.7 %copy.17 = bf16[128,512]{1,0:T(8,128)(2,1)} copy(bf16[128,512]{1,0:T(8,128)(2,1)S(1)} %get-tuple-element.3) | data formatting | bytes 262144
